TPU v7x, 32 devices: a whole 2x2x4 slice. The times are simulated.
32 devices in a mesh: sp: 16 (over z, y, x), tp: 2 (over core).
Axes of the slice: x: 2, y: 2, z: 4, core: 2. Of those that a mesh axis runs over, the one named last changes fastest.
Arguments:
- queries: bfloat16 [24576, 1024], P('sp', 'tp'), may hold values from -6 to 6
- forget_logit: bfloat16 [24576, 1024], P('sp', 'tp'), may hold values from -8 to 8
- value_rows: bfloat16 [24576, 1024], P('sp', 'tp'), may hold values from -10 to 10
- out_gate: bfloat16 [24576, 1024], P('sp', 'tp'), may hold values from -6 to 6
- floor_gap: float32 [1024], P('tp'), may hold values from 0 to 0.1, as said below
- head_gain: float32 [1024], P('tp'), may hold values from 0.1 to 1.9
- state_in: float32 [8, 128, 128], P('tp'), may hold values from -0.625 to 0.625
- out_weight: bfloat16 [1024, 2048], P('tp'), may hold values from -0.1875 to 0.1875
Outputs:
- projected: bfloat16 [24576, 2048], P(('sp', 'tp'))
- state_out: float32 [8, 16384], P('tp', 'sp')
Inputs may be any that keep to these rules, and one draw needn't show every extreme that they name: `floor_gap`: strictly between 0 and 0.1.
All inputs are finite; a program needn't handle non-finite values.
Results may differ from a plain program's by a relative error of at most 0.009.
Values may be sent and summed in bfloat16 or wider, within the bound.
A program may use at most 128 MiB of HBM per device.

v0:
```python
import jax
import jax.numpy as jnp
from jax import lax
from jax.sharding import PartitionSpec as P

BLOCK = 128


maximum_precision = lax.Precision.HIGHEST
epsilon = 1e-06


def entering(value, axis, join, neutral):
    count, mine = (lax.axis_size(axis), lax.axis_index(axis))
    pieces = jax.tree.map(lambda part: lax.all_gather(part, axis), value)
    so_far = jax.tree.map(
        lambda part, zero: jnp.full_like(part, 0) + jnp.asarray(zero, part.dtype), value, neutral
    )

    def hop(position, so_far):
        longer = join(so_far, jax.tree.map(lambda part: part[position], pieces))
        return jax.tree.map(lambda new, old: jnp.where(position < mine, new, old), longer, so_far)

    return lax.fori_loop(0, count - 1, hop, so_far)


def spread(block, axis, holder):
    block = jnp.where(lax.axis_index(axis) == holder, block, jnp.zeros_like(block))
    return lax.psum(block, axis)


def to_blocks(values, head_count):
    blocks = values.shape[0] // BLOCK
    return values.reshape(blocks, BLOCK, head_count, values.shape[1] // head_count)


def join_state(earlier, later):
    return (earlier[0] * later[0], later[0][..., None] * earlier[1] + later[1])


def per_device(
    queries, forget_logit, value_rows, out_gate, floor_gap, head_gain, state_in, out_weight
):
    span_rows = queries.shape[0]
    head_count = state_in.shape[0]
    key_gate = to_blocks(floor_gap * jax.nn.sigmoid(-forget_logit.astype(jnp.float32)), head_count)
    log_forget = jnp.log1p(-key_gate)
    reader = to_blocks(jax.nn.silu(queries.astype(jnp.float32)), head_count)
    written_update = to_blocks(value_rows.astype(jnp.float32), head_count)
    positions = jnp.arange(BLOCK)
    causal = positions[:, None] >= positions[None, :]
    lower_ones = causal.astype(jnp.float32)
    cumul = jnp.einsum("cs,nshk->nchk", lower_ones, log_forget, precision=maximum_precision)
    scaled_readout = reader * jnp.exp(cumul)
    key_scaled = key_gate * jnp.exp(-cumul)
    scores = jnp.einsum("nchk,nshk->nhcs", scaled_readout, key_scaled, precision=maximum_precision)
    scores = jnp.where(causal, scores, 0.0)
    within = jnp.einsum("nhcs,nshv->nchv", scores, written_update, precision=maximum_precision)
    block_log_decay = cumul[:, -1]
    decay_to_finish = key_gate * jnp.exp(block_log_decay[:, None] - cumul)
    segment_state = jnp.einsum(
        "nshk,nshv->nhkv", decay_to_finish, written_update, precision=maximum_precision
    )
    block_final_rows = jnp.cumsum(block_log_decay, axis=0)
    starts = block_final_rows - block_log_decay
    overall_log_decay = block_final_rows[-1]
    block_ids = jnp.arange(block_final_rows.shape[0])
    earlier_mask = (block_ids[:, None] > block_ids[None, :])[:, :, None, None]
    spacing = jnp.where(earlier_mask, starts[:, None] - block_final_rows[None, :], 0.0)
    carry_weight = jnp.where(earlier_mask, jnp.exp(spacing), 0.0)
    local_before = jnp.einsum(
        "jihk,ihkv->jhkv", carry_weight, segment_state, precision=maximum_precision
    )
    decay_dev = jnp.exp(overall_log_decay)
    state_dev = jnp.einsum(
        "lpt,lptr->ptr",
        jnp.exp(overall_log_decay[None] - block_final_rows),
        segment_state,
        precision=maximum_precision,
    )
    prefix_decay, prefix_state = entering(
        (decay_dev, state_dev),
        "sp",
        join_state,
        (jnp.ones_like(decay_dev), jnp.zeros_like(state_dev)),
    )
    incoming = prefix_decay[..., None] * state_in + prefix_state
    before = local_before + jnp.exp(starts)[..., None] * incoming[None]
    unscaled_output = within + jnp.einsum(
        "nchk,nhkv->nchv", scaled_readout, before, precision=maximum_precision
    )
    mean_square = jnp.mean(unscaled_output * unscaled_output, axis=-1, keepdims=True)
    gain_rows = head_gain.reshape(head_count, -1)
    normed = unscaled_output * lax.rsqrt(mean_square + epsilon) * gain_rows
    gating = jax.nn.silu(to_blocks(out_gate.astype(jnp.float32), head_count))
    gated = (normed * gating).astype(jnp.bfloat16).reshape(span_rows, -1)
    regrouped = lax.all_to_all(gated, "tp", split_axis=0, concat_axis=1, tiled=True)
    summed = jnp.dot(
        regrouped,
        lax.all_gather(out_weight, "tp", axis=0, tiled=True),
        preferred_element_type=jnp.float32,
    )
    projected = summed.astype(jnp.bfloat16)
    finished = (decay_dev[..., None] * incoming + state_dev).reshape(head_count, -1)
    whole_final = spread(finished.astype(jnp.bfloat16), "sp", lax.axis_size("sp") - 1).astype(
        finished.dtype
    )
    share = whole_final.shape[1] // lax.axis_size("sp")
    offset = lax.axis_index("sp") * share
    state_out = lax.dynamic_slice_in_dim(whole_final, offset, share, 1)
    return (projected, state_out)


def solution(mesh):
    placed = (
        P("sp", "tp"),
        P("sp", "tp"),
        P("sp", "tp"),
        P("sp", "tp"),
        P("tp"),
        P("tp"),
        P("tp", None, None),
        P("tp", None),
    )
    return jax.shard_map(
        per_device,
        mesh=mesh,
        in_specs=placed,
        out_specs=(P(("sp", "tp"), None), P("tp", "sp")),
        check_vma=False,
    )
```

profile of v0, /device:TPU:0, one launch (start us, length us, event | category | flops | bytes accessed | tf_op | source)
XLA Modules:
  0.0 276.8 jit_solution(8512602507941155407)
XLA Ops:
  7.2 3.9 %divide_multiply_fusion = f32[1536,512]{1,0:T(8,128)} fusion(bf16[1536,512]{1,0:T(8,128)(2,1)} %param.11, f32[512]{0:T(512)} %param.14), kind=kLoop, calls=%fused_computation.38 | loop fusion | flops 3145728 | bytes 4720640 | tf_op jit(solution)/shard_map/mul | solution.py:46
  11.1 3.1 %reshape.70 = f32[12,128,4,128]{3,2,1,0:T(4,128)S(1)} reshape(f32[1536,512]{1,0:T(8,128)} %divide_multiply_fusion) | data formatting | bytes 6291456 | tf_op jit(solution)/shard_map/reshape | solution.py:34
  15.9 1.8 fusion.32
  18.0 3.5 %reshape.71 = bf16[12,128,4,128]{3,2,1,0:T(4,128)(2,1)} reshape(bf16[1536,512]{1,0:T(8,128)(2,1)} %param.12) | data formatting | bytes 3145728 | tf_op jit(solution)/shard_map/reshape | solution.py:34
  21.5 5.2 %fusion.16 = f32[12,4,128,128]{3,2,1,0:T(8,128)S(1)} fusion(f32[12,128,4,128]{3,1,2,0:T(8,128)S(1)} %fusion.32, f32[12,128,4,128]{3,2,1,0:T(4,128)} %copy-done, f32[12,4,128]{2,1,0:T(4,128)S(1)} %bitcast.59, bf16[12,128,4,128]{3,2,1,0:T(4,128)(2,1)} %reshape.71), kind=kOutput, calls=%fused_computation.27 | convolution fusion | flops 1209532416 | bytes 11034624 | tf_op jit(solution)/shard_map/nshk,nshv->nhkv/dot_general | solution.py:61
  26.8 1.7 copy-done.2
  28.5 6.1 %fusion.1 = f32[4,128,1,128]{3,2,1,0:T(1,128)} fusion(f32[12,4,128,1]{0,3,2,1:T(1,128)S(1)} %copy.44, f32[12,4,128,128]{3,2,1,0:T(8,128)S(1)} %fusion.16), kind=kOutput, calls=%fused_computation.4 | convolution fusion | flops 9437184 | bytes 3432448 | tf_op jit(solution)/shard_map/lpt,lptr->ptr/dot_general | solution.py:75
  36.9 42.7 %all_gather.13 = f32[16,4,128]{2,1,0:T(4,128)S(1)} all-gather(f32[1,4,128]{2,1,0:T(4,128)S(1)} %get-tuple-element.153), channel_id=1, replica_groups=mesh['sp'=16,'tp'=2] {'sp'}, dimensions={0}, use_global_device_ids=true | all-gather | bytes 34816 | tf_op jit(solution)/shard_map/all_gather | solution.py:15
  81.3 4.0 %convert_multiply_fusion = f32[1536,512]{1,0:T(8,128)} fusion(bf16[1536,512]{1,0:T(8,128)(2,1)} %param.10), kind=kLoop, calls=%fused_computation.13 | loop fusion | flops 3932160 | bytes 4718592 | tf_op jit(solution)/shard_map/jit(silu)/mul | solution.py:48
  85.3 4.9 %reshape.69 = f32[12,128,4,128]{3,2,1,0:T(4,128)} reshape(f32[1536,512]{1,0:T(8,128)} %convert_multiply_fusion) | data formatting | bytes 6291456 | tf_op jit(solution)/shard_map/reshape | solution.py:34
  90.2 11.5 %fusion.22 = f32[12,4,128,128]{3,2,1,0:T(8,128)} fusion(f32[12,128,4,128]{3,1,2,0:T(8,128)S(1)} %fusion.32, f32[12,128,4,128]{3,2,1,0:T(4,128)} %copy-done, f32[12,128,4,128]{3,2,1,0:T(4,128)} %reshape.69), kind=kOutput, calls=%fused_computation.33 | convolution fusion | flops 1210318848 | bytes 12582912 | tf_op jit(solution)/shard_map/nchk,nshk->nhcs/dot_general | solution.py:56
  101.7 4.1 %reshape.75 = f32[12,128,4,128]{3,2,1,0:T(4,128)} reshape(bf16[1536,512]{1,0:T(8,128)(2,1)} %param.13) | data formatting | bytes 4718592 | tf_op jit(solution)/shard_map/reshape | solution.py:34
  105.8 4.9 %copy.39 = f32[12,128,4,128]{1,3,2,0:T(8,128)} copy(f32[12,128,4,128]{3,2,1,0:T(4,128)} %reshape.75) | data formatting | bytes 6291456 | tf_op jit(solution)/shard_map/reshape | solution.py:34
  110.6 2.4 all-gather.6.cloned.1.call-done
  113.1 18.1 %while.16 = (s32[]{:T(128)}, f32[4,128]{1,0:T(4,128)S(1)}, f32[4,128,128]{2,1,0:T(8,128)S(1)}, s32[]{:T(128)}, f32[16,4,128]{2,1,0:T(4,128)S(1)}, /*index=5*/f32[16,4,128,128]{3,2,1,0:T(8,128)}, s32[]{:T(128)}, s32[]{:T(128)}) while((s32[]{:T(128)}, f32[4,128]{1,0:T(4,128)S(1)}, f32[4,128,128]{2,1,0:T(8,128)S(1)}, s32[]{:T(128)}, ...), condition=%wide.region_2.3_spmd.clone, body=%wide.region_1.2_spmd.clone.sunk | while | flops 263684 | bytes 796787 | solution.py:24
  132.4 10.1 %bitcast_add_fusion.1 = f32[12,4,128,128]{3,0,2,1:T(8,128)S(1)} fusion(f32[4,128,128]{2,1,0:T(8,128)S(1)} %get-tuple-element.150, f32[12,4,128]{0,2,1:T(8,128)} %copy.36, f32[12,4,128]{0,2,1:T(8,128)} %copy.34, f32[12,4,128]{0,2,1:T(8,128)} %copy.33, pred[12,12]{1,0:T(8,128)(4,1)S(1)} %iota_compare_fusion.2, f32[12,4,128,128]{3,2,1,0:T(8,128)} %copy-done.2), kind=kOutput, calls=%fused_computation.8 | convolution fusion | flops 115040256 | bytes 6627472 | tf_op jit(solution)/shard_map/jihk,ihkv->jhkv/dot_general | solution.py:71
  142.6 6.5 %fusion.12 = f32[12,4,128,128]{3,2,1,0:T(8,128)S(1)} fusion(f32[12,4,128,128]{3,0,2,1:T(8,128)S(1)} %bitcast_add_fusion.1, f32[12,128,4,128]{3,2,1,0:T(4,128)S(1)} %copy-done.1, f32[12,128,4,128]{3,1,2,0:T(8,128)S(1)} %fusion.32), kind=kOutput, calls=%fused_computation.20 | convolution fusion | flops 1208745984 | bytes 12582912 | tf_op jit(solution)/shard_map/nchk,nhkv->nchv/dot_general | solution.py:89
  149.2 3.5 %multiply_reduce_fusion = (f32[12,128,4]{1,2,0:T(4,128)S(1)}, f32[12,128,4,128]{1,3,2,0:T(8,128)S(1)}) fusion(f32[12,4,128,128]{3,2,1,0:T(8,128)S(1)} %fusion.12, bf16[12,128,4,128]{3,2,1,0:T(4,128)(2,1)S(1)} %copy-done.3, f32[12,4,128,128]{3,2,1,0:T(8,128)S(1)} %copy-done.5, pred[128,128]{1,0:T(8,128)(4,1)S(1)} %copy-done.6), kind=kOutput, calls=%fused_computation.26 | convolution fusion | flops 1211099136 | bytes 11051008 | tf_op jit(solution)/shard_map/nhcs,nshv->nchv/dot_general | solution.py:58
  152.7 2.2 multiply_convert_fusion
  154.9 2.7 copy.40
  158.3 5.0 %all_to_all.19 = bf16[2,768,512]{2,1,0:T(8,128)(2,1)S(1)} all-to-all(bf16[2,768,512]{2,1,0:T(8,128)(2,1)S(1)} %all_to_all.14), channel_id=1, replica_groups=mesh['sp'=16,'tp'=2] {'tp'}, dimensions={0} | all-to-all | bytes 3145728 | tf_op jit(solution)/shard_map/all_to_all | solution.py:97
  164.8 7.0 %convolution_convert_fusion = bf16[768,2048]{1,0:T(8,128)(2,1)} fusion(bf16[768,1024]{0,1:T(8,128)(2,1)S(1)} %bitcast.53, bf16[1024,2048]{1,0:T(8,128)(2,1)} %all-gather.4.cloned.1.call-done), kind=kOutput, calls=%fused_computation.15 | convolution fusion | flops 3222798336 | bytes 8912896 | tf_op jit(solution)/shard_map/dot_general | solution.py:98
  171.8 97.2 %all-reduce.2.cloned.1.call-done = bf16[4,16384]{1,0:T(4,128)(2,1)} async-done(((bf16[4,16384]{1,0:T(4,128)(2,1)}), bf16[4,16384]{1,0:T(4,128)(2,1)}) %all-reduce.2.cloned.1.call-update) | async-done | bytes 131088 | tf_op jit(solution)/shard_map/psum | solution.py:29
  269.0 1.3 dynamic-slice_convert_fusion
  (72 shorter events, 27.0 us)
Async XLA Ops:
  7.2 105.9 %all-gather.6.cloned.1.call-start = ((), (), s32[]{:S(2)}) async-start(), calls=%async_computation.3 | async-start | bytes 4456448 | tf_op jit(solution)/shard_map/all_gather | solution.py:15
  14.3 1.7 copy-start
  26.7 1.7 copy-start.2
  34.6 130.2 %all-gather.4.cloned.1.call-start = ((), (), s32[]{:S(2)}) async-start(), calls=%async_computation.1 | async-start | bytes 6291456 | tf_op jit(solution)/shard_map/all_gather | solution.py:100
  35.3 233.7 %all-reduce.2.cloned.1.call-start = ((), (), s32[]{:S(2)}) async-start(), calls=%async_computation.2 | async-start | bytes 262144 | tf_op jit(solution)/shard_map/psum | solution.py:29
  132.4 10.1 %copy-start.1 = (f32[12,128,4,128]{3,2,1,0:T(4,128)S(1)}, f32[12,128,4,128]{3,2,1,0:T(4,128)}, u32[]{:S(2)}) copy-start(f32[12,128,4,128]{3,2,1,0:T(4,128)} %reshape.69) | copy-start | bytes 9437188
  142.6 6.6 %copy-start.3 = (bf16[12,128,4,128]{3,2,1,0:T(4,128)(2,1)S(1)}, bf16[12,128,4,128]{3,2,1,0:T(4,128)(2,1)}, u32[]{:S(2)}) copy-start(bf16[12,128,4,128]{3,2,1,0:T(4,128)(2,1)} %reshape.71) | copy-start | bytes 4718596
  142.6 6.6 %copy-start.5 = (f32[12,4,128,128]{3,2,1,0:T(8,128)S(1)}, f32[12,4,128,128]{3,2,1,0:T(8,128)}, u32[]{:S(2)}) copy-start(f32[12,4,128,128]{3,2,1,0:T(8,128)} %fusion.22) | copy-start | bytes 9437188
  142.6 6.6 %copy-start.6 = (pred[128,128]{1,0:T(8,128)(4,1)S(1)}, pred[128,128]{1,0:T(8,128)(4,1)}, u32[]{:S(2)}) copy-start(pred[128,128]{1,0:T(8,128)(4,1)} %iota_compare_fusion) | copy-start | bytes 49156
  149.1 3.5 %copy-start.4 = (f32[12,128,4,128]{1,3,2,0:T(8,128)S(1)}, f32[12,128,4,128]{1,3,2,0:T(8,128)}, u32[]{:S(2)}) copy-start(f32[12,128,4,128]{1,3,2,0:T(8,128)} %copy.39) | copy-start | bytes 9437188
  149.1 3.5 %copy-start.7 = (f32[512]{0:T(512)S(1)}, f32[512]{0:T(512)}, u32[]{:S(2)}) copy-start(f32[512]{0:T(512)} %param.15) | copy-start | bytes 6148
Sparse Core Ops, SparseCore 0:
  34.7 78.3 all-gather.5
  114.6 12.2 all-gather.3
  164.9 104.0 all-reduce.1
where the time goes:
time: 278 us; the launch traced here: 277 us
  waiting for transfers between devices  100 us (36%)
  matrix products  51.7 us (19%)
  blocking collectives  47.7 us (17%)
  other arithmetic  32 us (12%)
  local copies, waits for them, and re-layouts  30.4 us (11%)
  between operations  14 us (5%)
    psum x1, waiting for transfers between devices, spread(): return lax.psum(block, axis)  97.2 us
    all_gather x1, blocking collectives, entering(): pieces = jax.tree.map(lambda part: lax.all_gather(part, axis), value)  42.7 us
    reshape x5, local copies, waits for them, and re-layouts, to_blocks(): values.reshape(blocks, BLOCK, head_count, values.shape[1] // head_count)  20.5 us
    select_n x30, other arithmetic, hop(): jnp.where(position < mine, new, old)  17.6 us
    dot_general x1, matrix products, per_device(): jnp.einsum('nchk,nshk->nhcs', scaled_readout, key_scaled, precision=maxim...  11.5 us
    dot_general x1, matrix products, per_device(): jnp.einsum('jihk,ihkv->jhkv', carry_weight, segment_state, precision=maxi...  10.1 us
    dot_general x1, matrix products, per_device(): jnp.dot(regrouped, lax.all_gather(out_weight, 'tp', axis=0, tiled=True),...  7.04 us
    dot_general x1, matrix products, per_device(): jnp.einsum('nchk,nhkv->nchv', scaled_readout, before, precision=maximum_p...  6.52 us
  transfers between devices with their start and end apart: 3, of which 2 were waited for; matrix products, arithmetic and copies ran while one was open for 31% of the time, Pallas kernels for 0%

commit v1 on v0

v1 whole, which is shorter than its diff:
```python
import functools

import jax
import jax.numpy as jnp
from jax import lax
from jax.experimental import pallas as pl
from jax.experimental.pallas import tpu as pltpu
from jax.sharding import PartitionSpec as P

BLOCK = 128
TILE = 256
epsilon = 1e-06
MESH = pl.DeviceIdType.MESH
f32 = jnp.float32
bf16 = jnp.bfloat16


def nt(a, b):
    return lax.dot_general(a, b, (((1,), (1,)), ((), ())), preferred_element_type=f32)


def tn(a, b):
    return lax.dot_general(a, b, (((0,), (0,)), ((), ())), preferred_element_type=f32)


def nn(a, b):
    return jnp.dot(a, b, preferred_element_type=f32)


def kernel(
    dims,
    fl_any, v_any, q_any, og_any, gap_any, gain_any, st_any, w_any,
    out_any, so_any,
    fl, v, q, og, gap, gain, stin, wown, wpeer,
    ecum, kst, sbef, run, lt, es, raw, sg, qs2,
    sbuf, dmine, rbuf, dbuf, dall, tcol, obuf, ibuf, gsend, gown, gpeer, ob, so,
    in_sem, s1, r1, sd, rd, s2, r2, gs, gr, wsem, osem, so_sem,
):
    n, heads, blocks, kp, tiles = dims
    me = lax.axis_index("sp")
    core = lax.axis_index("tp")
    mate = 1 - core
    half = blocks // 2

    def local(i, src, dst):
        return pltpu.make_async_copy(src, dst, in_sem.at[i])

    loads = [
        local(0, fl_any, fl), local(1, v_any, v), local(2, gap_any, gap),
        local(3, q_any, q), local(4, og_any, og), local(5, gain_any, gain),
        local(6, st_any.at[:, pl.ds(me * kp, kp), :], stin), local(7, w_any, wown),
    ]
    for load in loads:
        load.start()

    barrier = pltpu.get_barrier_semaphore()

    def greet(d, c):
        pl.semaphore_signal(barrier, inc=1, device_id={"sp": lax.rem(me + d, n)}, device_id_type=MESH)
        return c

    lax.fori_loop(1, n, greet, 0)
    pl.semaphore_signal(barrier, inc=1, device_id={"tp": mate}, device_id_type=MESH)

    row = lax.broadcasted_iota(jnp.int32, (BLOCK, BLOCK), 0)
    col = lax.broadcasted_iota(jnp.int32, (BLOCK, BLOCK), 1)
    causal = row >= col
    lower = jnp.where(causal, 1.0, 0.0).astype(bf16)
    lower2 = jnp.concatenate([lower, lower], axis=1)

    run[...] = jnp.zeros_like(run)
    lt[...] = jnp.zeros_like(lt)
    dall[...] = jnp.zeros_like(dall)
    loads[0].wait()
    loads[1].wait()
    loads[2].wait()

    def first(b, c):
        rows = pl.ds(pl.multiple_of(b * BLOCK, BLOCK), BLOCK)
        es[b] = jnp.exp(lt[...])
        for h in range(heads):
            cols = slice(h * 128, (h + 1) * 128)
            x = fl[rows, cols].astype(f32)
            g = gap[:, cols] * (1.0 / (1.0 + jnp.exp(x)))
            lf = jnp.log1p(-g)
            hi = lf.astype(bf16)
            lo = (lf - hi.astype(f32)).astype(bf16)
            cum = nn(lower2, jnp.concatenate([hi, lo], axis=0))
            e = jnp.exp(cum)
            ks = g * jnp.exp(-cum)
            et = e[BLOCK - 1 : BLOCK, :]
            ecum[rows, cols] = e
            kst[rows, cols] = ks.astype(bf16)
            old = run[h]
            sbef[b, h] = old.astype(bf16)
            run[h] = old * et + tn(v[rows, cols], (ks * et).astype(bf16))
            lt[:, cols] = lt[:, cols] + cum[BLOCK - 1 : BLOCK, :]
        return c

    lax.fori_loop(0, blocks, first, 0)

    for h in range(heads):
        cols = slice(h * 128, (h + 1) * 128)
        sbuf[:, h] = run[h].T.reshape(n, kp, 128).astype(bf16)
        dmine[h : h + 1, :] = jnp.exp(lt[:, cols])

    pl.semaphore_wait(barrier, n)

    def state_copy(d):
        to = lax.rem(me + d, n)
        return pltpu.make_async_remote_copy(
            src_ref=sbuf.at[to], dst_ref=rbuf.at[me], send_sem=s1.at[d], recv_sem=r1.at[d],
            device_id={"sp": to}, device_id_type=MESH)

    def decay_copy(d):
        return pltpu.make_async_remote_copy(
            src_ref=dmine, dst_ref=dbuf.at[me], send_sem=sd.at[d], recv_sem=rd.at[d],
            device_id={"sp": lax.rem(me + d, n)}, device_id_type=MESH)

    def back_copy(d):
        to = lax.rem(me + d, n)
        return pltpu.make_async_remote_copy(
            src_ref=obuf.at[to], dst_ref=ibuf.at[me], send_sem=s2.at[d], recv_sem=r2.at[d],
            device_id={"sp": to}, device_id_type=MESH)

    def send_states(d, c):
        state_copy(d).start()
        decay_copy(d).start()
        return c

    lax.fori_loop(1, n, send_states, 0)
    weights = pltpu.make_async_remote_copy(
        src_ref=w_any, dst_ref=wpeer, send_sem=wsem.at[0], recv_sem=wsem.at[1],
        device_id={"tp": mate}, device_id_type=MESH)
    weights.start()
    rbuf[me] = sbuf[me]
    dbuf[me] = dmine[...]

    loads[3].wait()
    loads[4].wait()
    loads[5].wait()
    loads[6].wait()

    def second(b, c):
        rows = pl.ds(pl.multiple_of(b * BLOCK, BLOCK), BLOCK)
        start = es[b]
        for h in range(heads):
            cols = slice(h * 128, (h + 1) * 128)
            qv = q[rows, cols].astype(f32)
            scaled = qv * (1.0 / (1.0 + jnp.exp(-qv))) * ecum[rows, cols]
            qs = scaled.astype(bf16)
            qs2[rows, cols] = (scaled * start[:, cols]).astype(bf16)
            scores = jnp.where(causal, nt(qs, kst[rows, cols]), 0.0).astype(bf16)
            raw[rows, cols] = nn(scores, v[rows, cols]) + nt(qs, sbef[b, h])
            gv = og[rows, cols].astype(f32)
            sg[rows, cols] = gv * (1.0 / (1.0 + jnp.exp(-gv))) * gain[:, cols]
        return c

    lax.fori_loop(0, half, second, 0)

    def got_states(d, c):
        state_copy(d).wait_recv()
        decay_copy(d).wait_recv()
        return c

    lax.fori_loop(1, n, got_states, 0)

    def spread(j, c):
        dall[pl.ds(j * 8, heads), :] = dbuf[j]
        return c

    lax.fori_loop(0, n, spread, 0)
    tcol[...] = dall[...].T
    decays = tcol[pl.ds(me * kp, kp), :]
    for h in range(heads):
        state = stin[h]
        for j in range(n):
            obuf[j, h] = state.astype(bf16)
            state = decays[:, 8 * j + h : 8 * j + h + 1] * state + rbuf[j, h].astype(f32)
        for k in range(kp):
            so[h : h + 1, k * 128 : (k + 1) * 128] = state[k : k + 1, :]
    ibuf[me] = obuf[me]

    def send_back(d, c):
        back_copy(d).start()
        return c

    lax.fori_loop(1, n, send_back, 0)
    state_done = pltpu.make_async_copy(so, so_any, so_sem)
    state_done.start()

    lax.fori_loop(half, blocks, second, 0)

    def got_back(d, c):
        back_copy(d).wait_recv()
        return c

    lax.fori_loop(1, n, got_back, 0)
    incoming = [ibuf[:, h].astype(f32).reshape(n * kp, 128).astype(bf16) for h in range(heads)]

    def finish(rows, h):
        cols = slice(h * 128, (h + 1) * 128)
        out = raw[rows, cols] + nn(qs2[rows, cols], incoming[h])
        mean = jnp.mean(out * out, axis=-1, keepdims=True)
        return (out * lax.rsqrt(mean + epsilon) * sg[rows, cols]).astype(bf16)

    def gated_copy(i):
        rows = pl.ds(pl.multiple_of(i * BLOCK, BLOCK), BLOCK)
        return pltpu.make_async_remote_copy(
            src_ref=gsend.at[rows], dst_ref=gpeer.at[rows], send_sem=gs.at[i], recv_sem=gr.at[i],
            device_id={"tp": mate}, device_id_type=MESH)

    def theirs(i, c):
        rows = pl.ds(pl.multiple_of((mate * half + i) * BLOCK, BLOCK), BLOCK)
        to = pl.ds(pl.multiple_of(i * BLOCK, BLOCK), BLOCK)
        for h in range(heads):
            gsend[to, h * 128 : (h + 1) * 128] = finish(rows, h)

        @pl.when(i > 0)
        def _():
            gated_copy(i - 1).start()

        return c

    lax.fori_loop(0, half, theirs, 0)
    gated_copy(half - 1).start()

    def mine(i, c):
        rows = pl.ds(pl.multiple_of((core * half + i) * BLOCK, BLOCK), BLOCK)
        to = pl.ds(pl.multiple_of(i * BLOCK, BLOCK), BLOCK)
        for h in range(heads):
            gown[to, h * 128 : (h + 1) * 128] = finish(rows, h)
        return c

    lax.fori_loop(0, half, mine, 0)

    loads[7].wait()
    weights.wait()

    def got_gated(i, c):
        gated_copy(i).wait()
        return c

    lax.fori_loop(0, half, got_gated, 0)

    def out_copy(t):
        cols = pl.ds(pl.multiple_of(t * TILE, TILE), TILE)
        return pltpu.make_async_copy(ob.at[:, cols], out_any.at[:, cols], osem.at[t])

    def project(t, c):
        cols = pl.ds(pl.multiple_of(t * TILE, TILE), TILE)
        ob[:, cols] = (nn(gown[...], wown[:, cols]) + nn(gpeer[...], wpeer[:, cols])).astype(bf16)

        @pl.when(t > 0)
        def _():
            out_copy(t - 1).start()

        return c

    lax.fori_loop(0, tiles, project, 0)
    out_copy(tiles - 1).start()

    def sent(d, c):
        state_copy(d).wait_send()
        decay_copy(d).wait_send()
        back_copy(d).wait_send()
        return c

    lax.fori_loop(1, n, sent, 0)
    state_done.wait()

    def written(t, c):
        out_copy(t).wait()
        return c

    lax.fori_loop(0, tiles, written, 0)


def per_device(
    queries, forget_logit, value_rows, out_gate, floor_gap, head_gain, state_in, out_weight
):
    n = lax.axis_size("sp")
    rows, width = queries.shape
    heads = state_in.shape[0]
    depth = out_weight.shape[1]
    blocks = rows // BLOCK
    kp = 128 // n
    tiles = depth // TILE
    mine = rows // 2
    V = pltpu.VMEM
    D = pltpu.SemaphoreType.DMA
    scratch = [
        V((rows, width), bf16), V((rows, width), bf16), V((rows, width), bf16), V((rows, width), bf16),
        V((1, width), f32), V((1, width), f32), V((heads, kp, 128), f32),
        V((width, depth), bf16), V((width, depth), bf16),
        V((rows, width), f32), V((rows, width), bf16), V((blocks, heads, 128, 128), bf16),
        V((heads, 128, 128), f32), V((1, width), f32), V((blocks, 1, width), f32),
        V((rows, width), f32), V((rows, width), f32), V((rows, width), bf16),
        V((n, heads, kp, 128), bf16), V((heads, 128), f32), V((n, heads, kp, 128), bf16),
        V((n, heads, 128), f32), V((n * 8, 128), f32), V((128, n * 8), f32),
        V((n, heads, kp, 128), bf16), V((n, heads, kp, 128), bf16),
        V((mine, width), bf16), V((mine, width), bf16), V((mine, width), bf16),
        V((mine, depth), bf16), V((heads, kp * 128), f32),
        D((8,)), D((n,)), D((n,)), D((n,)), D((n,)), D((n,)), D((n,)),
        D((blocks // 2,)), D((blocks // 2,)), D((2,)), D((tiles,)), D(()),
    ]
    projected, state_out = pl.pallas_call(
        functools.partial(kernel, (n, heads, blocks, kp, tiles)),
        name="layer",
        out_shape=(
            jax.ShapeDtypeStruct((mine, depth), bf16),
            jax.ShapeDtypeStruct((heads, kp * 128), f32),
        ),
        in_specs=[pl.BlockSpec(memory_space=pl.ANY)] * 8,
        out_specs=(pl.BlockSpec(memory_space=pl.ANY),) * 2,
        scratch_shapes=scratch,
        compiler_params=pltpu.CompilerParams(
            collective_id=0, has_side_effects=True, vmem_limit_bytes=60 * 1024 * 1024
        ),
    )(
        forget_logit, value_rows, queries, out_gate,
        floor_gap.reshape(1, width), head_gain.reshape(1, width), state_in, out_weight,
    )
    return (projected, state_out)


def solution(mesh):
    placed = (
        P("sp", "tp"),
        P("sp", "tp"),
        P("sp", "tp"),
        P("sp", "tp"),
        P("tp"),
        P("tp"),
        P("tp", None, None),
        P("tp", None),
    )
    return jax.shard_map(
        per_device,
        mesh=mesh,
        in_specs=placed,
        out_specs=(P(("sp", "tp"), None), P("tp", "sp")),
        check_vma=False,
    )
```

time: 278 us -> 42.9 us (0.15)
  waiting for transfers between devices: 100 us -> 0 us
  matrix products: 51.7 us -> 0 us
  blocking collectives: 47.7 us -> 0 us
  Pallas kernels: 0 us -> 37.5 us
  other arithmetic: 32 us -> 0 us
  local copies, waits for them, and re-layouts: 30.4 us -> 4.58 us
  between operations: 14 us -> 0.65 us
    psum x1 -> x0, waiting for transfers between devices: 97.2 us -> none  [spread(): return lax.psum(block, axis)]
    dot_general x8 -> x0, matrix products: 51.7 us -> none  [the longest x1 11.5 us: per_device(): jnp.einsum('nchk,nshk->nhcs', scaled_readout, key_scaled, precision=maxim...]
    all_gather x1 -> x0, blocking collectives: 42.7 us -> none  [entering(): pieces = jax.tree.map(lambda part: lax.all_gather(part, axis), value)]
    pallas_call x0 -> x1, Pallas kernels: none -> 37.5 us  [per_device(): pl.pallas_call(functools.partial(kernel, (n, heads, blocks, kp, tiles)),...]
    reshape x5 -> x0, local copies, waits for them, and re-layouts: 20.5 us -> none  [to_blocks(): values.reshape(blocks, BLOCK, head_count, values.shape[1] // head_count)]
    select_n x30 -> x0, other arithmetic: 17.6 us -> none  [hop(): jnp.where(position < mine, new, old)]
    mul x2 -> x0, other arithmetic: 7.86 us -> none  [the longest x1 3.96 us: per_device(): reader = to_blocks(jax.nn.silu(queries.astype(jnp.float32)), head_count)]
    all_to_all x1 -> x0, blocking collectives: 5 us -> none  [per_device(): lax.all_to_all(gated, 'tp', split_axis=0, concat_axis=1, tiled=True)]
  transfers between devices with their start and end apart: 3 -> 0, of which waited for: 2 -> 0; matrix products, arithmetic and copies ran while one was open for 31% -> 0% of each run, Pallas kernels for 0% -> 0%
where the time goes in v1:
time: 42.9 us; the launch traced here: 42.7 us
  Pallas kernels  37.5 us (87%)
  local copies, waits for them, and re-layouts  4.58 us (11%)
  between operations  0.65 us (2%)
    pallas_call x1, Pallas kernels, per_device(): pl.pallas_call(functools.partial(kernel, (n, heads, blocks, kp, tiles)),...  37.5 us
    unnamed x4, local copies, waits for them, and re-layouts  4.58 us

profile of v1, /device:TPU:0, one launch (start us, length us, event | category | flops | bytes accessed | tf_op | source)
XLA Modules:
  0.0 42.7 jit_solution(4918786944578416926)
XLA Ops:
  0.6 37.5 %layer.1 = (bf16[768,2048]{1,0:T(8,128)(2,1)}, f32[4,1024]{1,0:T(4,128)}) custom-call(bf16[1536,512]{1,0:T(8,128)(2,1)} %fl_any.1, bf16[1536,512]{1,0:T(8,128)(2,1)} %v_any.1, bf16[1536,512]{1,0:T(8,128)(2,1)} %q_any.1, bf16[1536,512]{1,0:T(8,128)(2,1)} %og_any.1, f32[1,512]{1,0:T(1,128)} %bitcast.2, f32[1,512]{1,0:T(1,128)} %bitcast.3, ...), custom_call_target="tpu_custom_call" | custom-call | tf_op jit(solution)/shard_map/layer/pallas_call | solution.py:307
  38.1 0.0 copy-start
  38.1 4.0 %copy.12 = bf16[768,2048]{1,0:T(8,128)(2,1)} copy(bf16[768,2048]{1,0:T(8,128)(2,1)} %get-tuple-element.4) | data formatting | bytes 6291456
  42.1 0.0 copy-done
  42.1 0.6 %copy.13 = f32[4,1024]{1,0:T(4,128)} copy(f32[4,1024]{1,0:T(4,128)S(1)} %copy-done) | data formatting | bytes 32768
Async XLA Ops:
  38.1 4.0 %copy-start = (f32[4,1024]{1,0:T(4,128)S(1)}, f32[4,1024]{1,0:T(4,128)}, u32[]{:S(2)}) copy-start(f32[4,1024]{1,0:T(4,128)} %get-tuple-element.5) | copy-start | bytes 49156

commit v2 on v1

--- a/solution.py
+++ b/solution.py
@@ -8,11 +8,13 @@
 from jax.sharding import PartitionSpec as P
 
 BLOCK = 128
-TILE = 256
+TILE = 512
 epsilon = 1e-06
 MESH = pl.DeviceIdType.MESH
 f32 = jnp.float32
 bf16 = jnp.bfloat16
+VMEM_LAYER = 60 * 1024 * 1024
+LOG_TERMS = (0.248358778, 0.245560933, 0.33349572, 0.49999794, 1.0)
 
 
 def nt(a, b):
@@ -25,18 +27,26 @@
 
 def nn(a, b):
     return jnp.dot(a, b, preferred_element_type=f32)
+
+
+def log_keep(g):
+    series = LOG_TERMS[0]
+    for term in LOG_TERMS[1:]:
+        series = series * g + term
+    return -g * series
 
 
 def kernel(
     dims,
     fl_any, v_any, q_any, og_any, gap_any, gain_any, st_any, w_any,
-    out_any, so_any,
-    fl, v, q, og, gap, gain, stin, wown, wpeer,
-    ecum, kst, sbef, run, lt, es, raw, sg, qs2,
-    sbuf, dmine, rbuf, dbuf, dall, tcol, obuf, ibuf, gsend, gown, gpeer, ob, so,
-    in_sem, s1, r1, sd, rd, s2, r2, gs, gr, wsem, osem, so_sem,
+    gown_out, gpeer, wpeer, so_out,
+    fl, v, q, og, gap, gain, stin,
+    cumul, kg, sbef, run, lt, es, raw, sg, qs2,
+    hl, kst, dec, eb, qsc, gown, so,
+    sbuf, dmine, rbuf, dbuf, dall, tcol, obuf, ibuf, gsend,
+    in_sem, fl_sem, v_sem, s1, r1, sd, rd, s2, r2, gs, gr, wsem, gown_sem, so_sem,
 ):
-    n, heads, blocks, kp, tiles = dims
+    n, heads, blocks, kp = dims
     me = lax.axis_index("sp")
     core = lax.axis_index("tp")
     mate = 1 - core
@@ -45,13 +55,25 @@
     def local(i, src, dst):
         return pltpu.make_async_copy(src, dst, in_sem.at[i])
 
+    def early(b):
+        rows = pl.ds(pl.multiple_of(b * BLOCK, BLOCK), BLOCK)
+        return (
+            pltpu.make_async_copy(fl_any.at[rows], fl.at[rows], fl_sem.at[b]),
+            pltpu.make_async_copy(v_any.at[rows], v.at[rows], v_sem.at[b]),
+        )
+
+    def start_early(b, c):
+        for copy in early(b):
+            copy.start()
+        return c
+
+    gap_load = local(0, gap_any, gap)
+    gap_load.start()
+    lax.fori_loop(0, blocks, start_early, 0)
     loads = [
-        local(0, fl_any, fl), local(1, v_any, v), local(2, gap_any, gap),
-        local(3, q_any, q), local(4, og_any, og), local(5, gain_any, gain),
-        local(6, st_any.at[:, pl.ds(me * kp, kp), :], stin), local(7, w_any, wown),
+        local(1, q_any, q), local(2, og_any, og), local(3, gain_any, gain),
+        local(4, st_any.at[:, pl.ds(me * kp, kp), :], stin),
     ]
-    for load in loads:
-        load.start()
 
     barrier = pltpu.get_barrier_semaphore()
 
@@ -71,33 +93,63 @@
     run[...] = jnp.zeros_like(run)
     lt[...] = jnp.zeros_like(lt)
     dall[...] = jnp.zeros_like(dall)
-    loads[0].wait()
-    loads[1].wait()
-    loads[2].wait()
-
-    def first(b, c):
-        rows = pl.ds(pl.multiple_of(b * BLOCK, BLOCK), BLOCK)
-        es[b] = jnp.exp(lt[...])
+    gap_load.wait()
+
+    def block_rows(b):
+        return pl.ds(pl.multiple_of(b * BLOCK, BLOCK), BLOCK)
+
+    def gates(b, c):
+        rows = block_rows(b)
+        for copy in early(b):
+            copy.wait()
         for h in range(heads):
             cols = slice(h * 128, (h + 1) * 128)
             x = fl[rows, cols].astype(f32)
             g = gap[:, cols] * (1.0 / (1.0 + jnp.exp(x)))
-            lf = jnp.log1p(-g)
+            lf = log_keep(g)
             hi = lf.astype(bf16)
-            lo = (lf - hi.astype(f32)).astype(bf16)
-            cum = nn(lower2, jnp.concatenate([hi, lo], axis=0))
-            e = jnp.exp(cum)
-            ks = g * jnp.exp(-cum)
-            et = e[BLOCK - 1 : BLOCK, :]
-            ecum[rows, cols] = e
-            kst[rows, cols] = ks.astype(bf16)
+            kg[rows, cols] = g
+            hl[b, 0:BLOCK, cols] = hi
+            hl[b, BLOCK:, cols] = (lf - hi.astype(f32)).astype(bf16)
+        return c
+
+    def sums(b, c):
+        cumul[block_rows(b), :] = nn(lower2, hl[b])
+        return c
+
+    def decayed(b, c):
+        rows = block_rows(b)
+        es[b] = jnp.exp(lt[...])
+        last = cumul[pl.ds(b * BLOCK + BLOCK - 1, 1), :]
+        lt[...] = lt[...] + last
+        keep = jnp.exp(last)
+        eb[b] = keep
+        for h in range(heads):
+            cols = slice(h * 128, (h + 1) * 128)
+            keys = kg[rows, cols] * jnp.exp(-cumul[rows, cols])
+            kst[rows, cols] = keys.astype(bf16)
+            dec[rows, cols] = (keys * keep[:, cols]).astype(bf16)
+        return c
+
+    def states(b, c):
+        rows = block_rows(b)
+        for h in range(heads):
+            cols = slice(h * 128, (h + 1) * 128)
             old = run[h]
             sbef[b, h] = old.astype(bf16)
-            run[h] = old * et + tn(v[rows, cols], (ks * et).astype(bf16))
-            lt[:, cols] = lt[:, cols] + cum[BLOCK - 1 : BLOCK, :]
-        return c
-
-    lax.fori_loop(0, blocks, first, 0)
+            run[h] = old * eb[b][:, cols] + tn(v[rows, cols], dec[rows, cols])
+        return c
+
+    with jax.named_scope("gates"):
+        lax.fori_loop(0, blocks, gates, 0)
+    with jax.named_scope("sums"):
+        lax.fori_loop(0, blocks, sums, 0, unroll=2)
+    with jax.named_scope("decayed"):
+        lax.fori_loop(0, blocks, decayed, 0)
+    with jax.named_scope("states"):
+        lax.fori_loop(0, blocks, states, 0, unroll=2)
+    for load in loads:
+        load.start()
 
     for h in range(heads):
         cols = slice(h * 128, (h + 1) * 128)
@@ -136,34 +188,41 @@
     rbuf[me] = sbuf[me]
     dbuf[me] = dmine[...]
 
-    loads[3].wait()
-    loads[4].wait()
-    loads[5].wait()
-    loads[6].wait()
-
-    def second(b, c):
-        rows = pl.ds(pl.multiple_of(b * BLOCK, BLOCK), BLOCK)
+    for load in loads:
+        load.wait()
+
+    def reads(b, c):
+        rows = block_rows(b)
         start = es[b]
         for h in range(heads):
             cols = slice(h * 128, (h + 1) * 128)
-            qv = q[rows, cols].astype(f32)
-            scaled = qv * (1.0 / (1.0 + jnp.exp(-qv))) * ecum[rows, cols]
-            qs = scaled.astype(bf16)
+            hq = 0.5 * q[rows, cols].astype(f32)
+            scaled = (hq + hq * jnp.tanh(hq)) * jnp.exp(cumul[rows, cols])
+            qsc[rows, cols] = scaled.astype(bf16)
             qs2[rows, cols] = (scaled * start[:, cols]).astype(bf16)
+            hg = 0.5 * og[rows, cols].astype(f32)
+            sg[rows, cols] = (hg + hg * jnp.tanh(hg)) * gain[:, cols]
+        return c
+
+    def within(b, c):
+        rows = block_rows(b)
+        for h in range(heads):
+            cols = slice(h * 128, (h + 1) * 128)
+            qs = qsc[rows, cols]
             scores = jnp.where(causal, nt(qs, kst[rows, cols]), 0.0).astype(bf16)
             raw[rows, cols] = nn(scores, v[rows, cols]) + nt(qs, sbef[b, h])
-            gv = og[rows, cols].astype(f32)
-            sg[rows, cols] = gv * (1.0 / (1.0 + jnp.exp(-gv))) * gain[:, cols]
-        return c
-
-    lax.fori_loop(0, half, second, 0)
+        return c
+
+    with jax.named_scope("reads"):
+        lax.fori_loop(0, blocks, reads, 0)
 
     def got_states(d, c):
         state_copy(d).wait_recv()
         decay_copy(d).wait_recv()
         return c
 
-    lax.fori_loop(1, n, got_states, 0)
+    with jax.named_scope("wait1"):
+        lax.fori_loop(1, n, got_states, 0)
 
     def spread(j, c):
         dall[pl.ds(j * 8, heads), :] = dbuf[j]
@@ -186,16 +245,18 @@
         return c
 
     lax.fori_loop(1, n, send_back, 0)
-    state_done = pltpu.make_async_copy(so, so_any, so_sem)
+    state_done = pltpu.make_async_copy(so, so_out, so_sem)
     state_done.start()
 
-    lax.fori_loop(half, blocks, second, 0)
+    with jax.named_scope("within"):
+        lax.fori_loop(0, blocks, within, 0, unroll=3)
 
     def got_back(d, c):
         back_copy(d).wait_recv()
         return c
 
-    lax.fori_loop(1, n, got_back, 0)
+    with jax.named_scope("wait2"):
+        lax.fori_loop(1, n, got_back, 0)
     incoming = [ibuf[:, h].astype(f32).reshape(n * kp, 128).astype(bf16) for h in range(heads)]
 
     def finish(rows, h):
@@ -222,7 +283,8 @@
 
         return c
 
-    lax.fori_loop(0, half, theirs, 0)
+    with jax.named_scope("theirs"):
+        lax.fori_loop(0, half, theirs, 0, unroll=2)
     gated_copy(half - 1).start()
 
     def mine(i, c):
@@ -230,35 +292,29 @@
         to = pl.ds(pl.multiple_of(i * BLOCK, BLOCK), BLOCK)
         for h in range(heads):
             gown[to, h * 128 : (h + 1) * 128] = finish(rows, h)
-        return c
-
-    lax.fori_loop(0, half, mine, 0)
-
-    loads[7].wait()
+
+        @pl.when(i > 0)
+        def _():
+            own_copy(i - 1).start()
+
+        return c
+
+    def own_copy(i):
+        rows = block_rows(i)
+        return pltpu.make_async_copy(gown.at[rows], gown_out.at[rows], gown_sem.at[i])
+
+    with jax.named_scope("mine"):
+        lax.fori_loop(0, half, mine, 0, unroll=2)
+    own_copy(half - 1).start()
+
     weights.wait()
 
     def got_gated(i, c):
         gated_copy(i).wait()
+        own_copy(i).wait()
         return c
 
     lax.fori_loop(0, half, got_gated, 0)
-
-    def out_copy(t):
-        cols = pl.ds(pl.multiple_of(t * TILE, TILE), TILE)
-        return pltpu.make_async_copy(ob.at[:, cols], out_any.at[:, cols], osem.at[t])
-
-    def project(t, c):
-        cols = pl.ds(pl.multiple_of(t * TILE, TILE), TILE)
-        ob[:, cols] = (nn(gown[...], wown[:, cols]) + nn(gpeer[...], wpeer[:, cols])).astype(bf16)
-
-        @pl.when(t > 0)
-        def _():
-            out_copy(t - 1).start()
-
-        return c
-
-    lax.fori_loop(0, tiles, project, 0)
-    out_copy(tiles - 1).start()
 
     def sent(d, c):
         state_copy(d).wait_send()
@@ -269,11 +325,9 @@
     lax.fori_loop(1, n, sent, 0)
     state_done.wait()
 
-    def written(t, c):
-        out_copy(t).wait()
-        return c
-
-    lax.fori_loop(0, tiles, written, 0)
+def project(gown, gpeer, wown, wpeer, so, out, state):
+    out[...] = (nn(gown[...], wown[...]) + nn(gpeer[...], wpeer[...])).astype(bf16)
+    state[...] = so[...]
 
 
 def per_device(
@@ -292,35 +346,56 @@
     scratch = [
         V((rows, width), bf16), V((rows, width), bf16), V((rows, width), bf16), V((rows, width), bf16),
         V((1, width), f32), V((1, width), f32), V((heads, kp, 128), f32),
-        V((width, depth), bf16), V((width, depth), bf16),
-        V((rows, width), f32), V((rows, width), bf16), V((blocks, heads, 128, 128), bf16),
+        V((rows, width), f32), V((rows, width), f32), V((blocks, heads, 128, 128), bf16),
         V((heads, 128, 128), f32), V((1, width), f32), V((blocks, 1, width), f32),
         V((rows, width), f32), V((rows, width), f32), V((rows, width), bf16),
+        V((blocks, 2 * BLOCK, width), bf16), V((rows, width), bf16), V((rows, width), bf16),
+        V((blocks, 1, width), f32), V((rows, width), bf16), V((mine, width), bf16),
+        V((heads, kp * 128), f32),
         V((n, heads, kp, 128), bf16), V((heads, 128), f32), V((n, heads, kp, 128), bf16),
         V((n, heads, 128), f32), V((n * 8, 128), f32), V((128, n * 8), f32),
         V((n, heads, kp, 128), bf16), V((n, heads, kp, 128), bf16),
-        V((mine, width), bf16), V((mine, width), bf16), V((mine, width), bf16),
-        V((mine, depth), bf16), V((heads, kp * 128), f32),
-        D((8,)), D((n,)), D((n,)), D((n,)), D((n,)), D((n,)), D((n,)),
-        D((blocks // 2,)), D((blocks // 2,)), D((2,)), D((tiles,)), D(()),
+        V((mine, width), bf16),
+        D((5,)), D((blocks,)), D((blocks,)), D((n,)), D((n,)), D((n,)), D((n,)), D((n,)), D((n,)),
+        D((blocks // 2,)), D((blocks // 2,)), D((2,)), D((blocks // 2,)), D(()),
     ]
-    projected, state_out = pl.pallas_call(
-        functools.partial(kernel, (n, heads, blocks, kp, tiles)),
+    gown, gpeer, wpeer, so = pl.pallas_call(
+        functools.partial(kernel, (n, heads, blocks, kp)),
         name="layer",
         out_shape=(
-            jax.ShapeDtypeStruct((mine, depth), bf16),
+            jax.ShapeDtypeStruct((mine, width), bf16),
+            jax.ShapeDtypeStruct((mine, width), bf16),
+            jax.ShapeDtypeStruct((width, depth), bf16),
             jax.ShapeDtypeStruct((heads, kp * 128), f32),
         ),
-        in_specs=[pl.BlockSpec(memory_space=pl.ANY)] * 8,
-        out_specs=(pl.BlockSpec(memory_space=pl.ANY),) * 2,
+        in_specs=[pl.BlockSpec(memory_space=pltpu.HBM)] * 8,
+        out_specs=(pl.BlockSpec(memory_space=pltpu.HBM),) * 4,
         scratch_shapes=scratch,
         compiler_params=pltpu.CompilerParams(
-            collective_id=0, has_side_effects=True, vmem_limit_bytes=60 * 1024 * 1024
+            collective_id=0, has_side_effects=True, vmem_limit_bytes=VMEM_LAYER
         ),
     )(
         forget_logit, value_rows, queries, out_gate,
         floor_gap.reshape(1, width), head_gain.reshape(1, width), state_in, out_weight,
     )
+    whole = lambda t: (0, 0)
+    piece = lambda t: (0, t)
+    projected, state_out = pl.pallas_call(
+        project,
+        name="project",
+        grid=(tiles,),
+        out_shape=(
+            jax.ShapeDtypeStruct((mine, depth), bf16),
+            jax.ShapeDtypeStruct((heads, kp * 128), f32),
+        ),
+        in_specs=[
+            pl.BlockSpec((mine, width), whole), pl.BlockSpec((mine, width), whole),
+            pl.BlockSpec((width, TILE), piece), pl.BlockSpec((width, TILE), piece),
+            pl.BlockSpec((heads, kp * 128), whole),
+        ],
+        out_specs=(pl.BlockSpec((mine, TILE), piece), pl.BlockSpec((heads, kp * 128), whole)),
+        compiler_params=pltpu.CompilerParams(vmem_limit_bytes=VMEM_LAYER),
+    )(gown, gpeer, out_weight, wpeer, so)
     return (projected, state_out)
 
 

time: 42.9 us -> 34.8 us (0.81)
  local copies, waits for them, and re-layouts: 4.58 us -> 0 us
  Pallas kernels: 37.5 us -> 33.9 us
    unnamed x4 -> x0, local copies, waits for them, and re-layouts: 4.58 us -> none
    pallas_call x1 -> x2, Pallas kernels: 37.5 us -> 33.9 us  [the longest x1 26.8 us: per_device(): pl.pallas_call(functools.partial(kernel, (n, heads, blocks, kp)), name='l...]
where the time goes in v2:
time: 34.8 us; the launch traced here: 34.6 us
  Pallas kernels  33.9 us (97%)
  between operations  0.64 us (2%)
    pallas_call x1, Pallas kernels, per_device(): pl.pallas_call(functools.partial(kernel, (n, heads, blocks, kp)), name='l...  26.8 us
    pallas_call x1, Pallas kernels, per_device(): pl.pallas_call(project, name='project', grid=(tiles,), out_shape=(jax.Sha...  7.15 us

profile of v2, /device:TPU:0, one launch (start us, length us, event | category | flops | bytes accessed | tf_op | source)
XLA Modules:
  0.0 34.6 jit_solution(13941295950444487529)
XLA Ops:
  0.6 26.8 %layer.1 = (bf16[768,512]{1,0:T(8,128)(2,1)}, bf16[768,512]{1,0:T(8,128)(2,1)}, bf16[512,2048]{1,0:T(8,128)(2,1)}, f32[4,1024]{1,0:T(4,128)}) custom-call(bf16[1536,512]{1,0:T(8,128)(2,1)} %fl_any.1, bf16[1536,512]{1,0:T(8,128)(2,1)} %v_any.1, bf16[1536,512]{1,0:T(8,128)(2,1)} %q_any.1, bf16[1536,512]{1,0:T(8,128)(2,1)} %og_any.1, f32[1,512]{1,0:T(1,128)} %bitcast.2, ...), custom_call_target="tpu_custom_call" | custom-call | tf_op jit(solution)/shard_map/layer/pallas_call | solution.py:362
  27.4 7.2 %project.1 = (bf16[768,2048]{1,0:T(8,128)(2,1)}, f32[4,1024]{1,0:T(4,128)}) custom-call(bf16[768,512]{1,0:T(8,128)(2,1)} %get-tuple-element.6.gown, bf16[768,512]{1,0:T(8,128)(2,1)} %get-tuple-element.7.gpeer, bf16[512,2048]{1,0:T(8,128)(2,1)} %wown.1, bf16[512,2048]{1,0:T(8,128)(2,1)} %get-tuple-element.8.wpeer, f32[4,1024]{1,0:T(4,128)} %get-tuple-element.9.so), custom_call_target="tpu_custom_call" | custom-call | tf_op jit(solution)/shard_map/project/pallas_call | solution.py:383

commit v3 on v2

--- a/solution.py
+++ b/solution.py
@@ -143,11 +143,11 @@
     with jax.named_scope("gates"):
         lax.fori_loop(0, blocks, gates, 0)
     with jax.named_scope("sums"):
-        lax.fori_loop(0, blocks, sums, 0, unroll=2)
+        lax.fori_loop(0, blocks, sums, 0, unroll=4)
     with jax.named_scope("decayed"):
         lax.fori_loop(0, blocks, decayed, 0)
     with jax.named_scope("states"):
-        lax.fori_loop(0, blocks, states, 0, unroll=2)
+        lax.fori_loop(0, blocks, states, 0, unroll=4)
     for load in loads:
         load.start()
 
@@ -249,7 +249,7 @@
     state_done.start()
 
     with jax.named_scope("within"):
-        lax.fori_loop(0, blocks, within, 0, unroll=3)
+        lax.fori_loop(0, blocks, within, 0, unroll=6)
 
     def got_back(d, c):
         back_copy(d).wait_recv()
@@ -284,7 +284,7 @@
         return c
 
     with jax.named_scope("theirs"):
-        lax.fori_loop(0, half, theirs, 0, unroll=2)
+        lax.fori_loop(0, half, theirs, 0, unroll=3)
     gated_copy(half - 1).start()
 
     def mine(i, c):
@@ -304,7 +304,7 @@
         return pltpu.make_async_copy(gown.at[rows], gown_out.at[rows], gown_sem.at[i])
 
     with jax.named_scope("mine"):
-        lax.fori_loop(0, half, mine, 0, unroll=2)
+        lax.fori_loop(0, half, mine, 0, unroll=3)
     own_copy(half - 1).start()
 
     weights.wait()

time: 34.8 us -> 33 us (0.948)
  Pallas kernels: 33.9 us -> 32.1 us
    pallas_call x1, Pallas kernels: 26.8 us -> 25 us  [per_device(): pl.pallas_call(functools.partial(kernel, (n, heads, blocks, kp)), name='l...]
where the time goes in v3:
time: 33 us; the launch traced here: 32.8 us
  Pallas kernels  32.1 us (97%)
  between operations  0.64 us (2%)
    pallas_call x1, Pallas kernels, per_device(): pl.pallas_call(functools.partial(kernel, (n, heads, blocks, kp)), name='l...  25 us
    pallas_call x1, Pallas kernels, per_device(): pl.pallas_call(project, name='project', grid=(tiles,), out_shape=(jax.Sha...  7.15 us

profile of v3, /device:TPU:0, one launch (start us, length us, event | category | flops | bytes accessed | tf_op | source)
XLA Modules:
  0.0 32.8 jit_solution(9148201417364282958)
XLA Ops:
  0.6 25.0 %layer.1 = (bf16[768,512]{1,0:T(8,128)(2,1)}, bf16[768,512]{1,0:T(8,128)(2,1)}, bf16[512,2048]{1,0:T(8,128)(2,1)}, f32[4,1024]{1,0:T(4,128)}) custom-call(bf16[1536,512]{1,0:T(8,128)(2,1)} %fl_any.1, bf16[1536,512]{1,0:T(8,128)(2,1)} %v_any.1, bf16[1536,512]{1,0:T(8,128)(2,1)} %q_any.1, bf16[1536,512]{1,0:T(8,128)(2,1)} %og_any.1, f32[1,512]{1,0:T(1,128)} %bitcast.2, ...), custom_call_target="tpu_custom_call" | custom-call | tf_op jit(solution)/shard_map/layer/pallas_call | solution.py:362
  25.6 7.2 %project.1 = (bf16[768,2048]{1,0:T(8,128)(2,1)}, f32[4,1024]{1,0:T(4,128)}) custom-call(bf16[768,512]{1,0:T(8,128)(2,1)} %get-tuple-element.6.gown, bf16[768,512]{1,0:T(8,128)(2,1)} %get-tuple-element.7.gpeer, bf16[512,2048]{1,0:T(8,128)(2,1)} %wown.1, bf16[512,2048]{1,0:T(8,128)(2,1)} %get-tuple-element.8.wpeer, f32[4,1024]{1,0:T(4,128)} %get-tuple-element.9.so), custom_call_target="tpu_custom_call" | custom-call | tf_op jit(solution)/shard_map/project/pallas_call | solution.py:383
